TPU v7x, 512 devices: a whole 4x4x16 slice. The times are simulated.
512 devices in a mesh: sp: 64 (over z, y), tp: 8 (over x, core).
Axes of the slice: x: 4, y: 4, z: 16, core: 2. Of those that a mesh axis runs over, the one named last changes fastest.
Arguments:
- prompt: bfloat16 [64, 1024, 2048], P('sp', None, 'tp'), may hold values from -6 to 6
- new_input: bfloat16 [64, 2048], P('sp', 'tp'), may hold values from -140 to 140
- w_query: bfloat16 [2048, 2048], P('sp', 'tp'), may hold values from -0.21875 to 0.21875
- w_key: bfloat16 [2048, 2048], P('sp', 'tp'), may hold values from -0.125 to 0.125
- w_value: bfloat16 [2048, 2048], P('sp', 'tp'), may hold values from -0.125 to 0.125
- lam: float32 [16], P('tp'), may hold values from 0.3 to 0.8
- out_gain: float32 [128], replicated, may hold values from 0.1 to 1.9
Outputs:
- key_cache: bfloat16 [64, 1024, 2048], P('sp', None, 'tp')
- value_cache: bfloat16 [64, 1024, 2048], P('sp', None, 'tp')
- first_read: bfloat16 [64, 16, 128], P('sp', 'tp')
All inputs are finite; a program needn't handle non-finite values.
Results may differ from a plain program's by a relative error of at most 0.02.
The roundings to bfloat16 on the way count: a program that leaves them out, or rounds other values in their place, can miss the bound.
Values may be sent and summed in bfloat16 or wider, within the bound.
No kernel may reach another device: no remote copies, remote signals or barrier semaphores. Data moves between devices by JAX's collectives and lax.ppermute only.
A program may use at most 64 MiB of HBM per device.

v0:
```python
import jax
import jax.numpy as jnp
from jax import lax
from jax.sharding import Mesh
from jax.sharding import PartitionSpec as P

MAP_DIM = 64
VAL_DIM = 128
LEN = 1024
TP = ("tp_0", "tp_1")


rope_base = 500000.0
norm_eps = 1e-05


def sent_together(arrays, axis, dim, along):
    widths = [a.shape[along] for a in arrays]
    both = jnp.concatenate(arrays, axis=along)
    out = lax.all_gather(both, axis, axis=dim, tiled=True)
    return tuple(jnp.split(out, [sum(widths[:k]) for k in range(1, len(widths))], axis=along))


def from_everyone(value, axis):
    copies = jnp.broadcast_to(value, (lax.axis_size(axis), *value.shape))
    return lax.all_to_all(copies, axis, split_axis=0, concat_axis=0, tiled=True)


def laid_out(blocks, dim):
    blocks = jnp.moveaxis(blocks, 0, dim)
    dims = blocks.shape
    return blocks.reshape(*dims[:dim], dims[dim] * dims[dim + 1], *dims[dim + 2 :])


def whole_of(value, axes, dim):
    far, near = axes
    blocks = from_everyone(from_everyone(value, far), near)
    return laid_out(blocks.swapaxes(0, 1).reshape(-1, *value.shape), dim)


def sent_together_2(arrays, axis, dim, along):
    widths = [a.shape[along] for a in arrays]
    both = jnp.concatenate(arrays, axis=along)
    out = whole_of(both, axis, dim)
    return tuple(jnp.split(out, [sum(widths[:k]) for k in range(1, len(widths))], axis=along))


def rotate(vectors, angle):
    half = vectors.shape[-1] // 2
    cosine_table = jnp.cos(angle)
    sine = jnp.sin(angle)
    first = vectors[..., :half]
    second = vectors[..., half:]
    return jnp.concatenate(
        [first * cosine_table - second * sine, second * cosine_table + first * sine], axis=-1
    )


def inverse_freq():
    return rope_base ** (-(jnp.arange(MAP_DIM // 2, dtype=jnp.float32) * 2.0 / MAP_DIM))


def finish(mixed, lam, out_gain):
    diff = mixed[:, :, 0] - lam[None, :, None] * mixed[:, :, 1]
    normed = diff * lax.rsqrt(jnp.mean(diff * diff, axis=-1, keepdims=True) + norm_eps)
    return (normed * out_gain).astype(jnp.bfloat16)


def read_whole(query, keys, values, lam, out_gain):
    seqs, length, _ = keys.shape
    heads = lam.shape[0]
    key_maps = keys.reshape(seqs, length, heads, 2, MAP_DIM)
    value_heads = values.reshape(seqs, length, heads, VAL_DIM)
    attention_scores = jnp.einsum(
        "shmd,slhmd->shml", query, key_maps, preferred_element_type=jnp.float32
    ) * MAP_DIM ** (-0.5)
    weights = jax.nn.softmax(attention_scores, axis=-1)
    mixed = jnp.einsum(
        "shml,slhe->shme", weights, value_heads.astype(jnp.float32), precision=lax.Precision.HIGHEST
    )
    return finish(mixed, lam, out_gain)


def body(prompt, new_input, w_query, w_key, w_value, lam, out_gain):
    heads = lam.shape[0]
    seqs, count, _ = prompt.shape
    local_seqs = new_input.shape[0]
    inverse = inverse_freq()
    full_query, full_key, full_value = sent_together((w_query, w_key, w_value), "sp", 0, 1)
    whole_rows, whole_new_cache = sent_together_2(
        (prompt, new_input[:, None, :]), ("tp_0", "tp_1"), 2, 1
    )
    flat_rows = whole_rows.reshape(seqs * count, whole_rows.shape[2])
    key_sum = jnp.dot(flat_rows, full_key, preferred_element_type=jnp.float32)
    weighted_value_sum = jnp.dot(flat_rows, full_value, preferred_element_type=jnp.float32)
    query_sum = jnp.dot(whole_new_cache[:, 0, :], full_query, preferred_element_type=jnp.float32)
    positions = jnp.arange(count, dtype=jnp.float32)
    key_maps = rotate(
        key_sum.reshape(seqs, count, heads, 2, MAP_DIM), positions[:, None, None, None] * inverse
    )
    keys = key_maps.astype(jnp.bfloat16).reshape(seqs, count, heads * 2 * MAP_DIM)
    values = weighted_value_sum.astype(jnp.bfloat16).reshape(seqs, count, heads * VAL_DIM)
    query = rotate(
        query_sum.reshape(local_seqs, heads, 2, MAP_DIM), jnp.float32(LEN) * inverse
    ).astype(jnp.bfloat16)
    first_read = read_whole(query, keys, values, lam, out_gain)
    return (keys, values, first_read)


def solution(mesh):
    split = Mesh(mesh.devices.reshape(mesh.shape["sp"], 4, 2), ("sp", "tp_0", "tp_1"))
    in_specs = (P("sp", None, TP), P("sp", TP), P("sp", TP), P("sp", TP), P("sp", TP), P(TP), P())
    out_specs = (P("sp", None, TP), P("sp", None, TP), P("sp", TP, None))
    return jax.shard_map(body, mesh=split, in_specs=in_specs, out_specs=out_specs, check_vma=False)
```

profile of v0, /device:TPU:6, one launch (start us, length us, event | category | flops | bytes accessed | tf_op | source)
XLA Modules:
  0.0 180.6 jit_solution(9579178100986410921)
XLA Ops:
  7.2 0.0 all-gather.2.cloned.1.call-start
  7.2 1.4 pad_maximum_fusion.1
  8.6 1.1 maximum_bitcast_fusion
  9.7 1.5 broadcast_in_dim.7
  11.2 9.4 %all-to-all-start = ((bf16[4,1,1025,256]{3,2,1,0:T(8,128)(2,1)}), bf16[4,1,1025,256]{3,2,1,0:T(8,128)(2,1)S(1)}, u32[]{:S(2)}, u32[]{:S(2)}) async-start(bf16[4,1,1025,256]{3,2,1,0:T(8,128)(2,1)} %broadcast_in_dim.7), calls=%async_computation | async-start | bytes 4227072 | tf_op jit(solution)/shard_map/all_to_all | solution.py:26
  20.6 0.1 multiply_sine_fusion
  20.7 0.5 fusion.18
  21.2 19.2 %all-to-all-done = bf16[4,1,1025,256]{3,2,1,0:T(8,128)(2,1)S(1)} async-done(((bf16[4,1,1025,256]{3,2,1,0:T(8,128)(2,1)}), bf16[4,1,1025,256]{3,2,1,0:T(8,128)(2,1)S(1)}, u32[]{:S(2)}, u32[]{:S(2)}) %all-to-all-start) | async-done | bytes 2099232 | tf_op jit(solution)/shard_map/all_to_all | solution.py:26
  40.4 5.7 %copy.29 = bf16[4,1025,256]{2,0,1:T(4,128)(2,1)S(1)} copy(bf16[4,1025,256]{2,1,0:T(8,128)(2,1)S(1)} %bitcast.70) | data formatting | bytes 4198400 | tf_op jit(solution)/shard_map/all_to_all | solution.py:26
  46.1 4.0 %broadcast_in_dim.8 = bf16[2,4,1,1025,256]{4,1,3,2,0:T(4,128)(2,1)S(1)} broadcast(bf16[4,1025,256]{2,0,1:T(4,128)(2,1)S(1)} %copy.29), dimensions={1,3,4} | broadcast | bytes 6297600 | tf_op jit(solution)/shard_map/broadcast_in_dim | solution.py:25
  50.1 7.1 %all_to_all.13 = bf16[2,4,1,1025,256]{4,1,3,2,0:T(4,128)(2,1)S(1)} all-to-all(bf16[2,4,1,1025,256]{4,1,3,2,0:T(4,128)(2,1)S(1)} %broadcast_in_dim.8), channel_id=1, replica_groups=mesh['sp'=64,'tp_0'=4,'tp_1'=2] {'tp_1'}, dimensions={0} | all-to-all | bytes 8396800 | tf_op jit(solution)/shard_map/all_to_all | solution.py:26
  57.2 0.5 copy.30
  57.8 9.0 %copy.31 = bf16[1,1025,8,256]{3,2,1,0:T(8,128)(2,1)} copy(bf16[1,1025,8,256]{3,1,2,0:T(8,128)(2,1)S(1)} %bitcast.68) | data formatting | bytes 8396800 | tf_op jit(solution)/shard_map/transpose | solution.py:30
  66.8 7.5 %reshape.311 = bf16[1,1025,2048]{2,1,0:T(8,128)(2,1)} reshape(bf16[1,1025,8,256]{3,2,1,0:T(8,128)(2,1)} %copy.31) | data formatting | bytes 8396800 | tf_op jit(solution)/shard_map/reshape | solution.py:32
  74.2 84.9 %all-gather.2.cloned.1.call-done = bf16[2048,768]{1,0:T(8,128)(2,1)} async-done(((bf16[32,768]{1,0:T(8,128)(2,1)}), bf16[2048,768]{1,0:T(8,128)(2,1)}) %all-gather.2.cloned.1.call-update) | async-done | bytes 3145744 | tf_op jit(solution)/shard_map/all_gather | solution.py:20
  159.1 1.7 fusion.30
  160.8 0.6 copy.44
  161.5 0.6 copy.32
  162.1 1.4 fusion.21
  163.5 3.5 %fusion.6 = f32[1,1024,2,2,64]{1,4,3,2,0:T(8,128)S(1)} fusion(bf16[2,2,64,2048]{3,2,1,0:T(8,128)(2,1)S(1)} %bitcast.75, bf16[1,1025,2048]{2,1,0:T(8,128)(2,1)} %reshape.311), kind=kOutput, calls=%fused_computation.6 | convolution fusion | flops 1073741824 | bytes 6291456 | tf_op jit(solution)/shard_map/dot_general | solution.py:94
  167.0 0.1 fusion.25
  167.1 0.1 maximum_bitcast_fusion.1
  167.2 0.1 subtract_convert_fusion
  167.4 0.2 fusion.13
  167.6 0.1 fusion.27
  167.7 0.2 fusion.20
  167.9 2.5 %fusion.9 = bf16[1024,256]{0,1:T(8,128)(2,1)S(1)} fusion(bf16[1,1025,2048]{2,1,0:T(8,128)(2,1)S(1)} %bitcast.72, bf16[2048,768]{1,0:T(8,128)(2,1)} %all-gather.2.cloned.1.call-done), kind=kOutput, calls=%fused_computation.7 | convolution fusion | flops 1074003968 | bytes 5767168 | tf_op jit(solution)/shard_map/dot_general | solution.py:95
  170.4 0.6 convolution_bitcast_fusion
  171.0 0.2 multiply_reduce_fusion
  171.2 1.0 copy.36
  172.2 1.0 copy.37
  173.2 0.6 multiply_convert_fusion
  (14 shorter events, 0.1 us)
Async XLA Ops:
  7.2 151.9 %all-gather.2.cloned.1.call-start = ((), (), s32[]{:S(2)}) async-start(), calls=%async_computation.2 | async-start | bytes 3194880 | tf_op jit(solution)/shard_map/all_gather | solution.py:20
  11.2 29.2 %all-to-all-start = ((bf16[4,1,1025,256]{3,2,1,0:T(8,128)(2,1)}), bf16[4,1,1025,256]{3,2,1,0:T(8,128)(2,1)S(1)}, u32[]{:S(2)}, u32[]{:S(2)}) async-start(bf16[4,1,1025,256]{3,2,1,0:T(8,128)(2,1)} %broadcast_in_dim.7), calls=%async_computation | async-start | bytes 4227072 | tf_op jit(solution)/shard_map/all_to_all | solution.py:26
  162.1 5.7 %slice-start = ((s8[4227072]{0:T(1024)(128)(4,1)}), s8[4194304]{0:T(1024)(128)(4,1)S(1)}, s32[]{:S(2)}) async-start(s8[4227072]{0:T(1024)(128)(4,1)} %bitcast.71), calls=%async_computation.3 | async-start | bytes 8388608
  163.5 4.3 %slice-start.1 = ((s8[4227072]{0:T(1024)(128)(4,1)}), s8[32768]{0:T(1024)(128)(4,1)S(1)}, s32[]{:S(2)}) async-start(s8[4227072]{0:T(1024)(128)(4,1)} %bitcast.71), calls=%async_computation.4 | async-start | bytes 65536
  167.9 3.1 %copy-start.1 = (f32[2]{0:T(128)S(1)}, f32[2]{0:T(128)}, u32[]{:S(2)}) copy-start(f32[2]{0:T(128)} %param.12) | copy-start | bytes 28
  167.9 5.3 %copy-start = (f32[128]{0:T(128)S(1)}, f32[128]{0:T(128)}, u32[]{:S(2)}) copy-start(f32[128]{0:T(128)} %param.13) | copy-start | bytes 1540
Sparse Core Ops, SparseCore 0:
  11.5 147.5 all-gather.1
where the time goes:
time: 181 us
  waiting for transfers between devices  104 us (57%)
  local copies, waits for them, and re-layouts  33.2 us (18%)
  between operations  14.2 us (8%)
  starting transfers between devices  9.44 us (5%)
  matrix products  8.17 us (5%)
  blocking collectives  7.11 us (4%)
  other arithmetic  4.46 us (2%)
    all_gather x1, waiting for transfers between devices, sent_together(): out = lax.all_gather(both, axis, axis=dim, tiled=True)  84.9 us
    all_to_all x1, waiting for transfers between devices, from_everyone(): return lax.all_to_all(copies, axis, split_axis=0, concat_axis=0, tiled=True)  19.2 us
    all_to_all x1, starting transfers between devices, from_everyone(): return lax.all_to_all(copies, axis, split_axis=0, concat_axis=0, tiled=True)  9.4 us
    transpose x1, local copies, waits for them, and re-layouts, laid_out(): blocks = jnp.moveaxis(blocks, 0, dim)  8.97 us
    reshape x1, local copies, waits for them, and re-layouts, laid_out(): blocks.reshape(*dims[:dim], dims[dim] * dims[dim + 1], *dims[dim + 2:])  7.47 us
    all_to_all x1, blocking collectives, from_everyone(): return lax.all_to_all(copies, axis, split_axis=0, concat_axis=0, tiled=True)  7.11 us
    all_to_all x1, local copies, waits for them, and re-layouts, from_everyone(): return lax.all_to_all(copies, axis, split_axis=0, concat_axis=0, tiled=True)  5.68 us
    broadcast_in_dim x2, local copies, waits for them, and re-layouts, from_everyone(): copies = jnp.broadcast_to(value, (lax.axis_size(axis), *value.shape))  5.51 us
  transfers between devices with their start and end apart: 2, of which 2 were waited for; matrix products, arithmetic and copies ran while one was open for 17% of the time, Pallas kernels for 0%

commit v1 on v0

v1 whole, which is shorter than its diff:
```python
import functools

import jax
import jax.numpy as jnp
from jax import lax
from jax.experimental import pallas as pl
from jax.experimental.pallas import tpu as pltpu
from jax.sharding import Mesh
from jax.sharding import PartitionSpec as P

MAP_DIM = 64
VAL_DIM = 128
LEN = 1024
HALF = LEN // 2
PAD = 8
ROWS = 256
rope_base = 500000.0
norm_eps = 1e-05


def inverse_freq():
    return rope_base ** (-(jnp.arange(MAP_DIM // 2, dtype=jnp.float32) * 2.0 / MAP_DIM))


def tables(positions):
    angle = positions[:, None] * inverse_freq()
    cosine, sine = jnp.cos(angle), jnp.sin(angle)
    return jnp.tile(cosine, (1, 4)), jnp.tile(jnp.concatenate([-sine, sine], axis=1), (1, 2))


def shift(value, axis, by):
    n = lax.axis_size(axis)
    return lax.ppermute(value, axis, [(i, (i + by) % n) for i in range(n)])


def rotated(t, cosine, sine):
    lane = lax.broadcasted_iota(jnp.int32, t.shape, 1)
    partner = jnp.where(lane % MAP_DIM < MAP_DIM // 2, pltpu.roll(t, 128 - 32, 1), pltpu.roll(t, 32, 1))
    return t * cosine + partner * sine


def kernel(order, lam, own_p, far_p, own_c, far_c, weights, cos_t, sin_t, cos_q, sin_q, gain, keys, values, read, w):
    width = weights.shape[2]
    for j in range(8):
        t = order[j]
        for z in range(2):
            for y in range(4):
                row = pl.multiple_of((2 * t + z) * 32, 32)
                w[256 * j + 32 * (4 * z + y) : 256 * j + 32 * (4 * z + y) + 32, :] = weights[y, pl.ds(row, 32), :]

    def rows_of(lo, n):
        parts = [own_p[lo : lo + n, :]] + [far_p[k, lo : lo + n, :] for k in range(3)]
        parts += [own_c[lo : lo + n, :]] + [far_c[k, lo : lo + n, :] for k in range(3)]
        return jnp.concatenate(parts, axis=1)

    for m in range(LEN // ROWS):
        lo = m * ROWS
        both = jnp.dot(rows_of(lo, ROWS), w[:, 256:width], preferred_element_type=jnp.float32)
        cosine, sine = cos_t[lo : lo + ROWS, :], sin_t[lo : lo + ROWS, :]
        for h in range(2):
            part = both[:, 128 * h : 128 * h + 128]
            keys[lo : lo + ROWS, 128 * h : 128 * h + 128] = rotated(part, cosine, sine).astype(jnp.bfloat16)
        values[lo : lo + ROWS, :] = both[:, 256:512].astype(jnp.bfloat16)

    q = jnp.dot(rows_of(LEN, PAD), w[:, 0:256], preferred_element_type=jnp.float32)
    q = jnp.concatenate([rotated(q[:, 128 * h : 128 * h + 128], cos_q[...], sin_q[...]) for h in range(2)], axis=1)
    q = jnp.broadcast_to(q[0:1, :], (8, 256))
    row = lax.broadcasted_iota(jnp.int32, (8, 256), 0)
    lane = lax.broadcasted_iota(jnp.int32, (8, 256), 1)
    q = jnp.where(lane // MAP_DIM == row, q, 0.0).astype(jnp.bfloat16)
    scores = lax.dot_general(q, keys[...], (((1,), (1,)), ((), ())), preferred_element_type=jnp.float32)
    scores = scores * MAP_DIM ** (-0.5)
    e = jnp.exp(scores - jnp.max(scores, axis=1, keepdims=True))
    total = jnp.sum(e, axis=1, keepdims=True)
    high = e.astype(jnp.bfloat16)
    low = (e - high.astype(jnp.float32)).astype(jnp.bfloat16)
    v = values[...]
    mixed = jnp.dot(high, v, preferred_element_type=jnp.float32) + jnp.dot(low, v, preferred_element_type=jnp.float32)
    mixed = mixed / total
    for h in range(2):
        cols = mixed[:, VAL_DIM * h : VAL_DIM * h + VAL_DIM]
        diff = cols[2 * h : 2 * h + 1, :] - lam[h] * cols[2 * h + 1 : 2 * h + 2, :]
        normed = diff * lax.rsqrt(jnp.mean(diff * diff, axis=1, keepdims=True) + norm_eps)
        read[h : h + 1, :] = (normed * gain[...]).astype(jnp.bfloat16)


def compute(order, lam, arrays):
    vmem = pl.BlockSpec(memory_space=pltpu.VMEM)
    smem = pl.BlockSpec(memory_space=pltpu.SMEM)
    return pl.pallas_call(
        kernel,
        in_specs=[smem, smem] + [vmem] * len(arrays),
        out_specs=[vmem] * 3,
        out_shape=[
            jax.ShapeDtypeStruct((LEN, 256), jnp.bfloat16),
            jax.ShapeDtypeStruct((LEN, 256), jnp.bfloat16),
            jax.ShapeDtypeStruct((2, VAL_DIM), jnp.bfloat16),
        ],
        scratch_shapes=[pltpu.VMEM((2048, 768), jnp.bfloat16)],
        compiler_params=pltpu.CompilerParams(vmem_limit_bytes=40 * 1024 * 1024),
        name="project_and_read",
    )(order, lam, *arrays)


def body(prompt, new_input, w_query, w_key, w_value, lam, out_gain):
    own = jnp.concatenate([prompt[0], jnp.pad(new_input, ((0, PAD - 1), (0, 0)))], axis=0)
    one = shift(own, "x", 1)
    three = shift(own, "x", -1)
    two = jnp.concatenate([shift(own[:HALF], "x", 2), shift(own[HALF:], "x", -2)], axis=0)
    far = jnp.stack([one, two, three])
    own_c = shift(own, "c", 1)
    far_c = shift(far, "c", 1)

    mine = jnp.concatenate([w_query, w_key, w_value], axis=1)
    column = lax.all_gather(mine, "z", axis=0, tiled=True)
    weights = lax.all_to_all(jnp.broadcast_to(column, (4, *column.shape)), "y", 0, 0, tiled=True)

    ix, ic = lax.axis_index("x"), lax.axis_index("c")
    order = jnp.stack([2 * ((ix - d) % 4) + c for c in (ic, 1 - ic) for d in range(4)]).astype(jnp.int32)
    cos_t, sin_t = tables(jnp.arange(LEN, dtype=jnp.float32))
    cos_q, sin_q = tables(jnp.full((1,), LEN, jnp.float32))
    keys, values, read = compute(
        order, lam, (own, far, own_c, far_c, weights, cos_t, sin_t, cos_q, sin_q, out_gain[None])
    )
    return keys[None], values[None], read[None]


def solution(mesh):
    split = Mesh(mesh.devices.reshape(16, 4, 4, 2), ("z", "y", "x", "c"))
    sp, tp = ("z", "y"), ("x", "c")
    in_specs = (P(sp, None, tp), P(sp, tp), P(sp, tp), P(sp, tp), P(sp, tp), P(tp), P())
    out_specs = (P(sp, None, tp), P(sp, None, tp), P(sp, tp, None))
    return jax.shard_map(body, mesh=split, in_specs=in_specs, out_specs=out_specs, check_vma=False)
```

time: 181 us -> 105 us (0.58)
  waiting for transfers between devices: 104 us -> 15.2 us
  blocking collectives: 7.11 us -> 37.8 us
  local copies, waits for them, and re-layouts: 33.2 us -> 11.7 us
  starting transfers between devices: 9.44 us -> 25.8 us
  between operations: 14.2 us -> 0.91 us
  matrix products: 8.17 us -> 0 us
  Pallas kernels: 0 us -> 6.38 us
  other arithmetic: 4.46 us -> 6.3 us
    all_gather x1 -> x0, waiting for transfers between devices: 84.9 us -> none  [sent_together(): out = lax.all_gather(both, axis, axis=dim, tiled=True)]
    all_gather x0 -> x1, blocking collectives: none -> 37.8 us  [body(): column = lax.all_gather(mine, 'z', axis=0, tiled=True)]
    ppermute x0 -> x6, starting transfers between devices: none -> 21.3 us  [shift(): return lax.ppermute(value, axis, [(i, (i + by) % n) for i in range(n)])]
    transpose x2 -> x0, local copies, waits for them, and re-layouts: 9.52 us -> none  [the longest x1 8.97 us: laid_out(): blocks = jnp.moveaxis(blocks, 0, dim)]
    dot_general x5 -> x0, matrix products: 8.17 us -> none  [the longest x1 3.49 us: body(): key_sum = jnp.dot(flat_rows, full_key, preferred_element_type=jnp.float32)]
    reshape x1 -> x0, local copies, waits for them, and re-layouts: 7.47 us -> none  [laid_out(): blocks.reshape(*dims[:dim], dims[dim] * dims[dim + 1], *dims[dim + 2:])]
    all_to_all x1 -> x0, blocking collectives: 7.11 us -> none  [from_everyone(): return lax.all_to_all(copies, axis, split_axis=0, concat_axis=0, tiled=True)]
    pallas_call x0 -> x1, Pallas kernels: none -> 6.38 us  [compute(): pl.pallas_call(kernel, in_specs=[smem, smem] + [vmem] * len(arrays), out_...]
  transfers between devices with their start and end apart: 2 -> 7, of which waited for: 2 -> 1; matrix products, arithmetic and copies ran while one was open for 17% -> 13% of each run, Pallas kernels for 0% -> 0%
where the time goes in v1:
time: 105 us; the launch traced here: 104 us
  blocking collectives  37.8 us (36%)
  starting transfers between devices  25.8 us (25%)
  waiting for transfers between devices  15.2 us (14%)
  local copies, waits for them, and re-layouts  11.7 us (11%)
  Pallas kernels  6.38 us (6%)
  other arithmetic  6.3 us (6%)
    all_gather x1, blocking collectives, body(): column = lax.all_gather(mine, 'z', axis=0, tiled=True)  37.8 us
    ppermute x6, starting transfers between devices, shift(): return lax.ppermute(value, axis, [(i, (i + by) % n) for i in range(n)])  21.3 us
    all_to_all x1, waiting for transfers between devices, body(): lax.all_to_all(jnp.broadcast_to(column, (4, *column.shape)), 'y', 0, 0, t...  15.2 us
    pallas_call x1, Pallas kernels, compute(): pl.pallas_call(kernel, in_specs=[smem, smem] + [vmem] * len(arrays), out_...  6.38 us
    all_to_all x1, starting transfers between devices, body(): lax.all_to_all(jnp.broadcast_to(column, (4, *column.shape)), 'y', 0, 0, t...  4.46 us
    another operation x2, other arithmetic, body(): far = jnp.stack([one, two, three])  3.61 us
    another operation x4, local copies, waits for them, and re-layouts, tables(): jnp.tile(cosine, (1, 4))  2.99 us
    another operation x4, local copies, waits for them, and re-layouts, tables(): jnp.tile(jnp.concatenate([-sine, sine], axis=1), (1, 2))  2.97 us
  transfers between devices with their start and end apart: 7, of which 1 were waited for; matrix products, arithmetic and copies ran while one was open for 13% of the time, Pallas kernels for 0%

profile of v1, /device:TPU:6, one launch (start us, length us, event | category | flops | bytes accessed | tf_op | source)
XLA Modules:
  0.0 104.0 jit_solution(18313280759254075153)
XLA Ops:
  0.7 1.9 %fusion.1.own_p = bf16[1032,256]{1,0:T(8,128)(2,1)} fusion(bf16[1,256]{1,0:T(2,128)(2,1)} %param.8, bf16[1024,256]{1,0:T(8,128)(2,1)} %bitcast.26), kind=kLoop, calls=%fused_computation.3 | loop fusion | flops 1585152 | bytes 1053184 | tf_op jit(solution)/shard_map/concatenate | solution.py:106
  2.6 2.7 %collective-permute-start.3 = (bf16[1032,256]{1,0:T(8,128)(2,1)}, bf16[1032,256]{1,0:T(8,128)(2,1)}, u32[]{:S(2)}, u32[]{:S(2)}) collective-permute-start(bf16[1032,256]{1,0:T(8,128)(2,1)} %fusion.1.own_p), channel_id=1, source_target_pairs={{0,6},{2,0},{4,2},{6,4},{1,7},{3,1},{5,3},{7,5},{8,14},{10,8},{12,... | collective-permute-start | bytes 1585160 | tf_op jit(solution)/shard_map/ppermute | solution.py:33
  5.3 6.9 %collective-permute-start = (bf16[1032,256]{1,0:T(8,128)(2,1)}, bf16[1032,256]{1,0:T(8,128)(2,1)}, u32[]{:S(2)}, u32[]{:S(2)}) collective-permute-start(bf16[1032,256]{1,0:T(8,128)(2,1)} %fusion.1.own_p), channel_id=1, source_target_pairs={{0,2},{2,4},{4,6},{6,0},{1,3},{3,5},{5,7},{7,1},{8,10},{10,12},{12... | collective-permute-start | bytes 1585160 | tf_op jit(solution)/shard_map/ppermute | solution.py:33
  12.3 1.0 slice.12
  13.3 3.4 %collective-permute-start.2 = (bf16[520,256]{1,0:T(8,128)(2,1)S(1)}, bf16[520,256]{1,0:T(8,128)(2,1)}, u32[]{:S(2)}, u32[]{:S(2)}) collective-permute-start(bf16[520,256]{1,0:T(8,128)(2,1)S(1)} %slice.12), channel_id=1, source_target_pairs={{0,4},{2,6},{4,0},{6,2},{1,5},{3,7},{5,1},{7,3},{8,12},{10,14},{12... | collective-permute-start | bytes 798728 | tf_op jit(solution)/shard_map/ppermute | solution.py:33
  16.6 0.7 slice_bitcast_fusion
  17.4 4.0 %collective-permute-start.1 = (bf16[512,256]{1,0:T(8,128)(2,1)}, bf16[512,256]{1,0:T(8,128)(2,1)}, u32[]{:S(2)}, u32[]{:S(2)}) collective-permute-start(bf16[512,256]{1,0:T(8,128)(2,1)} %slice_bitcast_fusion), channel_id=1, source_target_pairs={{0,4},{2,6},{4,0},{6,2},{1,5},{3,7},{5,1},{7,3},{8,12},{10,14},{12... | collective-permute-start | bytes 786440 | tf_op jit(solution)/shard_map/ppermute | solution.py:33
  21.4 37.8 %all_gather.3 = bf16[512,768]{1,0:T(8,128)(2,1)S(1)} all-gather(bf16[32,768]{1,0:T(8,128)(2,1)S(1)} %pad_maximum_fusion.2), channel_id=1, replica_groups=mesh['z'=16,'y'=4,'x'=4,'c'=2] {'z'}, dimensions={0}, use_global_device_ids=true | all-gather | bytes 835584 | tf_op jit(solution)/shard_map/all_gather | solution.py:115
  59.1 1.8 %broadcast_in_dim.18 = bf16[4,512,768]{2,1,0:T(8,128)(2,1)} broadcast(bf16[512,768]{1,0:T(8,128)(2,1)S(1)} %all_gather.3), dimensions={1,2} | broadcast | bytes 3932160 | tf_op jit(solution)/shard_map/broadcast_in_dim | solution.py:116
  61.0 4.5 %all-to-all-start = ((bf16[4,512,768]{2,1,0:T(8,128)(2,1)}), bf16[4,512,768]{2,1,0:T(8,128)(2,1)S(1)}, u32[]{:S(2)}, u32[]{:S(2)}) async-start(bf16[4,512,768]{2,1,0:T(8,128)(2,1)} %broadcast_in_dim.18), calls=%async_computation | async-start | bytes 6291456 | tf_op jit(solution)/shard_map/all_to_all | solution.py:116
  65.5 0.0 collective-permute-done.1
  65.5 0.0 collective-permute-done.2
  65.5 1.1 %maximum_bitcast_fusion = bf16[1,1032,256]{2,1,0:T(8,128)(2,1)S(1)} fusion(bf16[520,256]{1,0:T(8,128)(2,1)} %collective-permute-done.2, bf16[512,256]{1,0:T(8,128)(2,1)} %collective-permute-done.1), kind=kLoop, calls=%fused_computation.4 | loop fusion | flops 1056768 | bytes 1056768 | tf_op jit(solution)/shard_map/stack | solution.py:110
  66.6 2.5 %pad_maximum_fusion.far_p = bf16[3,1032,256]{2,1,0:T(8,128)(2,1)} fusion(bf16[1,1032,256]{2,1,0:T(8,128)(2,1)} %bitcast.12, bf16[1,1032,256]{2,1,0:T(8,128)(2,1)S(1)} %maximum_bitcast_fusion, bf16[1,1032,256]{2,1,0:T(8,128)(2,1)} %bitcast.9), kind=kLoop, calls=%fused_computation | loop fusion | flops 1585152 | bytes 3170304 | tf_op jit(solution)/shard_map/stack | solution.py:110
  69.1 1.9 %collective-permute-start.5 = (bf16[3,1032,256]{2,1,0:T(8,128)(2,1)}, bf16[3,1032,256]{2,1,0:T(8,128)(2,1)}, u32[]{:S(2)}, u32[]{:S(2)}) collective-permute-start(bf16[3,1032,256]{2,1,0:T(8,128)(2,1)} %pad_maximum_fusion.far_p), channel_id=1, source_target_pairs={{0,1},{1,0},{2,3},{3,2},{4,5},{5,4},{6,7},{7,6},{8,9},{9,8},{10,11... | collective-permute-start | bytes 4755464 | tf_op jit(solution)/shard_map/ppermute | solution.py:33
  71.0 2.4 %collective-permute-start.4 = (bf16[1032,256]{1,0:T(8,128)(2,1)}, bf16[1032,256]{1,0:T(8,128)(2,1)}, u32[]{:S(2)}, u32[]{:S(2)}) collective-permute-start(bf16[1032,256]{1,0:T(8,128)(2,1)} %fusion.1.own_p), channel_id=1, source_target_pairs={{0,1},{1,0},{2,3},{3,2},{4,5},{5,4},{6,7},{7,6},{8,9},{9,8},{10,11... | collective-permute-start | bytes 1585160 | tf_op jit(solution)/shard_map/ppermute | solution.py:33
  73.4 0.5 fusion.4
  74.1 0.8 tile.18
  74.9 2.1 %copy.10.cos_t = f32[1024,128]{1,0:T(8,128)} copy(f32[1024,128]{0,1:T(8,128)} %bitcast.24) | data formatting | bytes 1048576 | tf_op jit(solution)/shard_map/tile | solution.py:28
  77.0 0.9 tile.40
  77.9 2.0 %copy.11.sin_t = f32[1024,128]{1,0:T(8,128)} copy(f32[1024,128]{0,1:T(8,128)} %bitcast.25) | data formatting | bytes 1048576 | tf_op jit(solution)/shard_map/tile | solution.py:28
  80.0 0.1 tile.43.cos_q
  80.0 0.1 multiply_sine_fusion
  80.1 0.1 maximum_bitcast_fusion.1
  80.2 0.1 tile.46.sin_q
  80.3 0.1 stack.47.order
  80.3 0.0 collective-permute-done.4.own_c
  80.4 0.0 collective-permute-done.5.far_c
  80.4 15.2 %all-to-all-done.weights = bf16[4,512,768]{2,1,0:T(8,128)(2,1)S(1)} async-done(((bf16[4,512,768]{2,1,0:T(8,128)(2,1)}), bf16[4,512,768]{2,1,0:T(8,128)(2,1)S(1)}, u32[]{:S(2)}, u32[]{:S(2)}) %all-to-all-start) | async-done | bytes 3145760 | tf_op jit(solution)/shard_map/all_to_all | solution.py:116
  95.5 1.0 %copy-done = f32[1024,128]{1,0:T(8,128)S(1)} copy-done((f32[1024,128]{1,0:T(8,128)S(1)}, f32[1024,128]{1,0:T(8,128)}, u32[]{:S(2)}) %copy-start) | copy-done | bytes 524312
  96.6 1.0 copy-done.1
  97.6 6.4 %project_and_read.1 = (bf16[1024,256]{1,0:T(8,128)(2,1)}, bf16[1024,256]{1,0:T(8,128)(2,1)}, bf16[2,128]{1,0:T(2,128)(2,1)}) custom-call(s32[8]{0:T(128)S(1)} %stack.47.order, f32[2]{0:T(128)S(1)} %copy-done.2, bf16[1032,256]{1,0:T(8,128)(2,1)} %fusion.1.own_p, bf16[3,1032,256]{2,1,0:T(8,128)(2,1)} %pad_maximum_fusion.far_p, ...), custom_call_target="tpu_custom_call" | custom-call | tf_op jit(solution)/shard_map/project_and_read/pallas_call | solution.py:90
  (22 shorter events, 0.1 us)
Async XLA Ops:
  0.6 16.0 %copy-start.4 = (bf16[1,1024,256]{2,1,0:T(8,128)(2,1)S(1)}, bf16[1,1024,256]{2,1,0:T(8,128)(2,1)}, u32[]{:S(2)}) copy-start(bf16[1,1024,256]{2,1,0:T(8,128)(2,1)} %param.7) | copy-start | bytes 1572868
  0.6 20.7 %copy-start.5 = (bf16[32,256]{1,0:T(8,128)(2,1)S(1)}, bf16[32,256]{1,0:T(8,128)(2,1)}, u32[]{:S(2)}) copy-start(bf16[32,256]{1,0:T(8,128)(2,1)} %param.11) | copy-start | bytes 49156
  0.7 20.7 %copy-start.6 = (bf16[32,256]{1,0:T(8,128)(2,1)S(1)}, bf16[32,256]{1,0:T(8,128)(2,1)}, u32[]{:S(2)}) copy-start(bf16[32,256]{1,0:T(8,128)(2,1)} %param.10) | copy-start | bytes 49156
  0.7 20.7 %copy-start.7 = (bf16[32,256]{1,0:T(8,128)(2,1)S(1)}, bf16[32,256]{1,0:T(8,128)(2,1)}, u32[]{:S(2)}) copy-start(bf16[32,256]{1,0:T(8,128)(2,1)} %param.9) | copy-start | bytes 49156
  2.6 63.9 %collective-permute-start.3 = (bf16[1032,256]{1,0:T(8,128)(2,1)}, bf16[1032,256]{1,0:T(8,128)(2,1)}, u32[]{:S(2)}, u32[]{:S(2)}) collective-permute-start(bf16[1032,256]{1,0:T(8,128)(2,1)} %fusion.1.own_p), channel_id=1, source_target_pairs={{0,6},{2,0},{4,2},{6,4},{1,7},{3,1},{5,3},{7,5},{8,14},{10,8},{12,... | collective-permute-start | bytes 1585160 | tf_op jit(solution)/shard_map/ppermute | solution.py:33
  5.3 61.2 %collective-permute-start = (bf16[1032,256]{1,0:T(8,128)(2,1)}, bf16[1032,256]{1,0:T(8,128)(2,1)}, u32[]{:S(2)}, u32[]{:S(2)}) collective-permute-start(bf16[1032,256]{1,0:T(8,128)(2,1)} %fusion.1.own_p), channel_id=1, source_target_pairs={{0,2},{2,4},{4,6},{6,0},{1,3},{3,5},{5,7},{7,1},{8,10},{10,12},{12... | collective-permute-start | bytes 1585160 | tf_op jit(solution)/shard_map/ppermute | solution.py:33
  13.3 52.2 %collective-permute-start.2 = (bf16[520,256]{1,0:T(8,128)(2,1)S(1)}, bf16[520,256]{1,0:T(8,128)(2,1)}, u32[]{:S(2)}, u32[]{:S(2)}) collective-permute-start(bf16[520,256]{1,0:T(8,128)(2,1)S(1)} %slice.12), channel_id=1, source_target_pairs={{0,4},{2,6},{4,0},{6,2},{1,5},{3,7},{5,1},{7,3},{8,12},{10,14},{12... | collective-permute-start | bytes 798728 | tf_op jit(solution)/shard_map/ppermute | solution.py:33
  17.4 48.1 %collective-permute-start.1 = (bf16[512,256]{1,0:T(8,128)(2,1)}, bf16[512,256]{1,0:T(8,128)(2,1)}, u32[]{:S(2)}, u32[]{:S(2)}) collective-permute-start(bf16[512,256]{1,0:T(8,128)(2,1)} %slice_bitcast_fusion), channel_id=1, source_target_pairs={{0,4},{2,6},{4,0},{6,2},{1,5},{3,7},{5,1},{7,3},{8,12},{10,14},{12... | collective-permute-start | bytes 786440 | tf_op jit(solution)/shard_map/ppermute | solution.py:33
  61.0 34.5 %all-to-all-start = ((bf16[4,512,768]{2,1,0:T(8,128)(2,1)}), bf16[4,512,768]{2,1,0:T(8,128)(2,1)S(1)}, u32[]{:S(2)}, u32[]{:S(2)}) async-start(bf16[4,512,768]{2,1,0:T(8,128)(2,1)} %broadcast_in_dim.18), calls=%async_computation | async-start | bytes 6291456 | tf_op jit(solution)/shard_map/all_to_all | solution.py:116
  69.1 11.3 %collective-permute-start.5 = (bf16[3,1032,256]{2,1,0:T(8,128)(2,1)}, bf16[3,1032,256]{2,1,0:T(8,128)(2,1)}, u32[]{:S(2)}, u32[]{:S(2)}) collective-permute-start(bf16[3,1032,256]{2,1,0:T(8,128)(2,1)} %pad_maximum_fusion.far_p), channel_id=1, source_target_pairs={{0,1},{1,0},{2,3},{3,2},{4,5},{5,4},{6,7},{7,6},{8,9},{9,8},{10,11... | collective-permute-start | bytes 4755464 | tf_op jit(solution)/shard_map/ppermute | solution.py:33
  71.0 9.3 %collective-permute-start.4 = (bf16[1032,256]{1,0:T(8,128)(2,1)}, bf16[1032,256]{1,0:T(8,128)(2,1)}, u32[]{:S(2)}, u32[]{:S(2)}) collective-permute-start(bf16[1032,256]{1,0:T(8,128)(2,1)} %fusion.1.own_p), channel_id=1, source_target_pairs={{0,1},{1,0},{2,3},{3,2},{4,5},{5,4},{6,7},{7,6},{8,9},{9,8},{10,11... | collective-permute-start | bytes 1585160 | tf_op jit(solution)/shard_map/ppermute | solution.py:33
  74.9 20.6 %copy-start.2 = (f32[2]{0:T(128)S(1)}, f32[2]{0:T(128)}, u32[]{:S(2)}) copy-start(f32[2]{0:T(128)} %lam.1) | copy-start | bytes 28
  74.9 20.6 %copy-start.3 = (f32[128]{0:T(128)S(1)}, f32[128]{0:T(128)}, u32[]{:S(2)}) copy-start(f32[128]{0:T(128)} %param.13) | copy-start | bytes 1540
  95.5 1.0 %copy-start = (f32[1024,128]{1,0:T(8,128)S(1)}, f32[1024,128]{1,0:T(8,128)}, u32[]{:S(2)}) copy-start(f32[1024,128]{1,0:T(8,128)} %copy.10.cos_t) | copy-start | bytes 1572868
  96.6 1.0 %copy-start.1 = (f32[1024,128]{1,0:T(8,128)S(1)}, f32[1024,128]{1,0:T(8,128)}, u32[]{:S(2)}) copy-start(f32[1024,128]{1,0:T(8,128)} %copy.11.sin_t) | copy-start | bytes 1572868

commit v2 on v1

--- a/solution.py
+++ b/solution.py
@@ -1,5 +1,3 @@
-import functools
-
 import jax
 import jax.numpy as jnp
 from jax import lax
@@ -8,10 +6,10 @@
 from jax.sharding import Mesh
 from jax.sharding import PartitionSpec as P
 
+
 MAP_DIM = 64
 VAL_DIM = 128
 LEN = 1024
-HALF = LEN // 2
 PAD = 8
 ROWS = 256
 rope_base = 500000.0
@@ -23,9 +21,10 @@
 
 
 def tables(positions):
-    angle = positions[:, None] * inverse_freq()
-    cosine, sine = jnp.cos(angle), jnp.sin(angle)
-    return jnp.tile(cosine, (1, 4)), jnp.tile(jnp.concatenate([-sine, sine], axis=1), (1, 2))
+    inverse = inverse_freq()
+    angle = positions[:, None] * jnp.tile(inverse, 4)[None, :]
+    sign = jnp.where(jnp.arange(128) % MAP_DIM < MAP_DIM // 2, -1.0, 1.0)
+    return jnp.cos(angle), jnp.sin(angle) * sign[None, :]
 
 
 def shift(value, axis, by):
@@ -39,7 +38,7 @@
     return t * cosine + partner * sine
 
 
-def kernel(order, lam, own_p, far_p, own_c, far_c, weights, cos_t, sin_t, cos_q, sin_q, gain, keys, values, read, w):
+def kernel(order, lam, a0, a1, a2, a3, b0, b1, b2, b3, weights, cos_t, sin_t, cos_q, sin_q, gain, keys, values, read, w):
     width = weights.shape[2]
     for j in range(8):
         t = order[j]
@@ -49,9 +48,7 @@
                 w[256 * j + 32 * (4 * z + y) : 256 * j + 32 * (4 * z + y) + 32, :] = weights[y, pl.ds(row, 32), :]
 
     def rows_of(lo, n):
-        parts = [own_p[lo : lo + n, :]] + [far_p[k, lo : lo + n, :] for k in range(3)]
-        parts += [own_c[lo : lo + n, :]] + [far_c[k, lo : lo + n, :] for k in range(3)]
-        return jnp.concatenate(parts, axis=1)
+        return jnp.concatenate([p[lo : lo + n, :] for p in (a0, a1, a2, a3, b0, b1, b2, b3)], axis=1)
 
     for m in range(LEN // ROWS):
         lo = m * ROWS
@@ -103,24 +100,22 @@
 
 
 def body(prompt, new_input, w_query, w_key, w_value, lam, out_gain):
-    own = jnp.concatenate([prompt[0], jnp.pad(new_input, ((0, PAD - 1), (0, 0)))], axis=0)
-    one = shift(own, "x", 1)
-    three = shift(own, "x", -1)
-    two = jnp.concatenate([shift(own[:HALF], "x", 2), shift(own[HALF:], "x", -2)], axis=0)
-    far = jnp.stack([one, two, three])
-    own_c = shift(own, "c", 1)
-    far_c = shift(far, "c", 1)
-
     mine = jnp.concatenate([w_query, w_key, w_value], axis=1)
     column = lax.all_gather(mine, "z", axis=0, tiled=True)
     weights = lax.all_to_all(jnp.broadcast_to(column, (4, *column.shape)), "y", 0, 0, tiled=True)
+
+    own = jnp.concatenate([prompt[0], jnp.pad(new_input, ((0, PAD - 1), (0, 0)))], axis=0)
+    near = [own]
+    for d in range(1, 4):
+        near.append(shift(own, "x", d))
+    partner = [shift(p, "c", 1) for p in near]
 
     ix, ic = lax.axis_index("x"), lax.axis_index("c")
     order = jnp.stack([2 * ((ix - d) % 4) + c for c in (ic, 1 - ic) for d in range(4)]).astype(jnp.int32)
     cos_t, sin_t = tables(jnp.arange(LEN, dtype=jnp.float32))
     cos_q, sin_q = tables(jnp.full((1,), LEN, jnp.float32))
     keys, values, read = compute(
-        order, lam, (own, far, own_c, far_c, weights, cos_t, sin_t, cos_q, sin_q, out_gain[None])
+        order, lam, (*near, *partner, weights, cos_t, sin_t, cos_q, sin_q, out_gain[None])
     )
     return keys[None], values[None], read[None]
 

time: 105 us -> 89.7 us (0.85)
  the two profiles are of different devices: /device:TPU:6 before, /device:TPU:1 now
where the time goes in v2:
time: 89.7 us; the launch traced here: 89.2 us
  starting transfers between devices  38.1 us (42%)
  blocking collectives  33.9 us (38%)
  Pallas kernels  6.37 us (7%)
  other arithmetic  5.6 us (6%)
  local copies, waits for them, and re-layouts  4.28 us (5%)
    all_gather x1, blocking collectives, body(): column = lax.all_gather(mine, 'z', axis=0, tiled=True)  33.9 us
    ppermute x7, starting transfers between devices, shift(): return lax.ppermute(value, axis, [(i, (i + by) % n) for i in range(n)])  33.8 us
    pallas_call x1, Pallas kernels, compute(): pl.pallas_call(kernel, in_specs=[smem, smem] + [vmem] * len(arrays), out_...  6.37 us
    all_to_all x1, starting transfers between devices, body(): lax.all_to_all(jnp.broadcast_to(column, (4, *column.shape)), 'y', 0, 0, t...  4.31 us
    mul x2, other arithmetic, tables(): return (jnp.cos(angle), jnp.sin(angle) * sign[None, :])  2.83 us
    unnamed x10, local copies, waits for them, and re-layouts  2.09 us
    concatenate x1, other arithmetic, body(): jnp.concatenate([prompt[0], jnp.pad(new_input, ((0, PAD - 1), (0, 0)))],...  1.9 us
    broadcast_in_dim x1, local copies, waits for them, and re-layouts, body(): jnp.broadcast_to(column, (4, *column.shape))  1.85 us
  transfers between devices with their start and end apart: 8, of which 0 were waited for; matrix products, arithmetic and copies ran while one was open for 6% of the time, Pallas kernels for 0%

profile of v2, /device:TPU:1, one launch (start us, length us, event | category | flops | bytes accessed | tf_op | source)
XLA Modules:
  0.0 89.2 jit_solution(5723040764411073122)
XLA Ops:
  0.6 0.8 pad_maximum_fusion
  1.4 33.9 %all_gather.3 = bf16[512,768]{1,0:T(8,128)(2,1)S(1)} all-gather(bf16[32,768]{1,0:T(8,128)(2,1)S(1)} %pad_maximum_fusion), channel_id=1, replica_groups=mesh['z'=16,'y'=4,'x'=4,'c'=2] {'z'}, dimensions={0}, use_global_device_ids=true | all-gather | bytes 835584 | tf_op jit(solution)/shard_map/all_gather | solution.py:104
  35.3 1.8 %broadcast_in_dim.32 = bf16[4,512,768]{2,1,0:T(8,128)(2,1)} broadcast(bf16[512,768]{1,0:T(8,128)(2,1)S(1)} %all_gather.3), dimensions={1,2} | broadcast | bytes 3932160 | tf_op jit(solution)/shard_map/broadcast_in_dim | solution.py:105
  37.1 4.3 %all-to-all-start = ((bf16[4,512,768]{2,1,0:T(8,128)(2,1)}), bf16[4,512,768]{2,1,0:T(8,128)(2,1)S(1)}, u32[]{:S(2)}, u32[]{:S(2)}) async-start(bf16[4,512,768]{2,1,0:T(8,128)(2,1)} %broadcast_in_dim.32), calls=%async_computation | async-start | bytes 6291456 | tf_op jit(solution)/shard_map/all_to_all | solution.py:105
  41.4 0.0 copy-done.4
  41.4 1.9 %fusion.1.a0 = bf16[1032,256]{1,0:T(8,128)(2,1)} fusion(bf16[1,256]{1,0:T(2,128)(2,1)S(1)} %copy-done.4, bf16[1024,256]{1,0:T(8,128)(2,1)} %bitcast.14), kind=kLoop, calls=%fused_computation.2 | loop fusion | flops 1585152 | bytes 1053184 | tf_op jit(solution)/shard_map/concatenate | solution.py:107
  43.3 3.1 %collective-permute-start = (bf16[1032,256]{1,0:T(8,128)(2,1)}, bf16[1032,256]{1,0:T(8,128)(2,1)}, u32[]{:S(2)}, u32[]{:S(2)}) collective-permute-start(bf16[1032,256]{1,0:T(8,128)(2,1)} %fusion.1.a0), channel_id=1, source_target_pairs={{0,2},{2,4},{4,6},{6,0},{1,3},{3,5},{5,7},{7,1},{8,10},{10,12},{12... | collective-permute-start | bytes 1585160 | tf_op jit(solution)/shard_map/ppermute | solution.py:32
  46.5 4.4 %collective-permute-start.1 = (bf16[1032,256]{1,0:T(8,128)(2,1)}, bf16[1032,256]{1,0:T(8,128)(2,1)}, u32[]{:S(2)}, u32[]{:S(2)}) collective-permute-start(bf16[1032,256]{1,0:T(8,128)(2,1)} %fusion.1.a0), channel_id=1, source_target_pairs={{0,4},{2,6},{4,0},{6,2},{1,5},{3,7},{5,1},{7,3},{8,12},{10,14},{12... | collective-permute-start | bytes 1585160 | tf_op jit(solution)/shard_map/ppermute | solution.py:32
  50.8 3.1 %collective-permute-start.2 = (bf16[1032,256]{1,0:T(8,128)(2,1)}, bf16[1032,256]{1,0:T(8,128)(2,1)}, u32[]{:S(2)}, u32[]{:S(2)}) collective-permute-start(bf16[1032,256]{1,0:T(8,128)(2,1)} %fusion.1.a0), channel_id=1, source_target_pairs={{0,6},{2,0},{4,2},{6,4},{1,7},{3,1},{5,3},{7,5},{8,14},{10,8},{12,... | collective-permute-start | bytes 1585160 | tf_op jit(solution)/shard_map/ppermute | solution.py:32
  53.9 10.8 %collective-permute-start.3 = (bf16[1032,256]{1,0:T(8,128)(2,1)}, bf16[1032,256]{1,0:T(8,128)(2,1)}, u32[]{:S(2)}, u32[]{:S(2)}) collective-permute-start(bf16[1032,256]{1,0:T(8,128)(2,1)} %fusion.1.a0), channel_id=1, source_target_pairs={{0,1},{1,0},{2,3},{3,2},{4,5},{5,4},{6,7},{7,6},{8,9},{9,8},{10,11... | collective-permute-start | bytes 1585160 | tf_op jit(solution)/shard_map/ppermute | solution.py:32
  64.7 0.0 collective-permute-done.a1
  64.8 5.0 %collective-permute-start.4 = (bf16[1032,256]{1,0:T(8,128)(2,1)}, bf16[1032,256]{1,0:T(8,128)(2,1)}, u32[]{:S(2)}, u32[]{:S(2)}) collective-permute-start(bf16[1032,256]{1,0:T(8,128)(2,1)} %collective-permute-done.a1), channel_id=1, source_target_pairs={{0,1},{1,0},{2,3},{3,2},{4,5},{5,4},{6,7},{7,6},{8,9},{9,8},{10,11... | collective-permute-start | bytes 1585160 | tf_op jit(solution)/shard_map/ppermute | solution.py:32
  69.7 0.0 collective-permute-done.1.a2
  69.7 5.6 %collective-permute-start.5 = (bf16[1032,256]{1,0:T(8,128)(2,1)}, bf16[1032,256]{1,0:T(8,128)(2,1)}, u32[]{:S(2)}, u32[]{:S(2)}) collective-permute-start(bf16[1032,256]{1,0:T(8,128)(2,1)} %collective-permute-done.1.a2), channel_id=1, source_target_pairs={{0,1},{1,0},{2,3},{3,2},{4,5},{5,4},{6,7},{7,6},{8,9},{9,8},{10,11... | collective-permute-start | bytes 1585160 | tf_op jit(solution)/shard_map/ppermute | solution.py:32
  75.4 0.0 collective-permute-done.2.a3
  75.4 1.9 %collective-permute-start.6 = (bf16[1032,256]{1,0:T(8,128)(2,1)}, bf16[1032,256]{1,0:T(8,128)(2,1)}, u32[]{:S(2)}, u32[]{:S(2)}) collective-permute-start(bf16[1032,256]{1,0:T(8,128)(2,1)} %collective-permute-done.2.a3), channel_id=1, source_target_pairs={{0,1},{1,0},{2,3},{3,2},{4,5},{5,4},{6,7},{7,6},{8,9},{9,8},{10,11... | collective-permute-start | bytes 1585160 | tf_op jit(solution)/shard_map/ppermute | solution.py:32
  77.5 0.1 mul.80
  77.5 0.1 cos.10.cos_q
  77.6 0.1 sin.20
  77.7 0.1 stack.35.order
  77.8 2.8 %sine_multiply_fusion = (f32[1024,128]{1,0:T(8,128)}, f32[1024,128]{1,0:T(8,128)}) fusion(f32[128]{0:T(128)S(1)} %compare_select_fusion.1, f32[128]{0:T(128)S(1)} %mul.80), kind=kLoop, calls=%fused_computation.3 | loop fusion | flops 262144 | bytes 1049600 | tf_op jit(solution)/shard_map/mul | solution.py:27
  80.6 0.0 collective-permute-done.3.b0
  80.6 0.0 collective-permute-done.4.b1
  80.6 0.0 collective-permute-done.5.b2
  80.7 0.0 collective-permute-done.6.b3
  80.7 0.0 all-to-all-done.weights
  80.7 0.0 copy-done.2
  80.7 0.0 copy-done.3
  80.7 0.0 copy-start
  80.7 1.0 %copy-done = f32[1024,128]{1,0:T(8,128)S(1)} copy-done((f32[1024,128]{1,0:T(8,128)S(1)}, f32[1024,128]{1,0:T(8,128)}, u32[]{:S(2)}) %copy-start) | copy-done | bytes 524312
  81.7 1.0 %copy-done.1 = f32[1024,128]{1,0:T(8,128)S(1)} copy-done((f32[1024,128]{1,0:T(8,128)S(1)}, f32[1024,128]{1,0:T(8,128)}, u32[]{:S(2)}) %copy-start.1) | copy-done | bytes 524312
  82.8 6.4 %project_and_read.1 = (bf16[1024,256]{1,0:T(8,128)(2,1)}, bf16[1024,256]{1,0:T(8,128)(2,1)}, bf16[2,128]{1,0:T(2,128)(2,1)}) custom-call(s32[8]{0:T(128)S(1)} %stack.35.order, f32[2]{0:T(128)S(1)} %copy-done.2, bf16[1032,256]{1,0:T(8,128)(2,1)} %fusion.1.a0, bf16[1032,256]{1,0:T(8,128)(2,1)} %collective-permute-done.a1, ...), custom_call_target="tpu_custom_call" | custom-call | tf_op jit(solution)/shard_map/project_and_read/pallas_call | solution.py:87
  (12 shorter events, 0.1 us)
Async XLA Ops:
  37.1 4.3 %copy-start.4 = (bf16[1,256]{1,0:T(2,128)(2,1)S(1)}, bf16[1,256]{1,0:T(2,128)(2,1)}, u32[]{:S(2)}) copy-start(bf16[1,256]{1,0:T(2,128)(2,1)} %param.8) | copy-start | bytes 1540
  37.1 43.6 %all-to-all-start = ((bf16[4,512,768]{2,1,0:T(8,128)(2,1)}), bf16[4,512,768]{2,1,0:T(8,128)(2,1)S(1)}, u32[]{:S(2)}, u32[]{:S(2)}) async-start(bf16[4,512,768]{2,1,0:T(8,128)(2,1)} %broadcast_in_dim.32), calls=%async_computation | async-start | bytes 6291456 | tf_op jit(solution)/shard_map/all_to_all | solution.py:105
  41.4 39.2 %copy-start.2 = (f32[2]{0:T(128)S(1)}, f32[2]{0:T(128)}, u32[]{:S(2)}) copy-start(f32[2]{0:T(128)} %lam.1) | copy-start | bytes 28
  41.4 39.3 %copy-start.3 = (f32[128]{0:T(128)S(1)}, f32[128]{0:T(128)}, u32[]{:S(2)}) copy-start(f32[128]{0:T(128)} %param.13) | copy-start | bytes 1540
  43.3 21.4 %collective-permute-start = (bf16[1032,256]{1,0:T(8,128)(2,1)}, bf16[1032,256]{1,0:T(8,128)(2,1)}, u32[]{:S(2)}, u32[]{:S(2)}) collective-permute-start(bf16[1032,256]{1,0:T(8,128)(2,1)} %fusion.1.a0), channel_id=1, source_target_pairs={{0,2},{2,4},{4,6},{6,0},{1,3},{3,5},{5,7},{7,1},{8,10},{10,12},{12... | collective-permute-start | bytes 1585160 | tf_op jit(solution)/shard_map/ppermute | solution.py:32
  46.5 23.3 %collective-permute-start.1 = (bf16[1032,256]{1,0:T(8,128)(2,1)}, bf16[1032,256]{1,0:T(8,128)(2,1)}, u32[]{:S(2)}, u32[]{:S(2)}) collective-permute-start(bf16[1032,256]{1,0:T(8,128)(2,1)} %fusion.1.a0), channel_id=1, source_target_pairs={{0,4},{2,6},{4,0},{6,2},{1,5},{3,7},{5,1},{7,3},{8,12},{10,14},{12... | collective-permute-start | bytes 1585160 | tf_op jit(solution)/shard_map/ppermute | solution.py:32
  50.8 24.6 %collective-permute-start.2 = (bf16[1032,256]{1,0:T(8,128)(2,1)}, bf16[1032,256]{1,0:T(8,128)(2,1)}, u32[]{:S(2)}, u32[]{:S(2)}) collective-permute-start(bf16[1032,256]{1,0:T(8,128)(2,1)} %fusion.1.a0), channel_id=1, source_target_pairs={{0,6},{2,0},{4,2},{6,4},{1,7},{3,1},{5,3},{7,5},{8,14},{10,8},{12,... | collective-permute-start | bytes 1585160 | tf_op jit(solution)/shard_map/ppermute | solution.py:32
  53.9 26.8 %collective-permute-start.3 = (bf16[1032,256]{1,0:T(8,128)(2,1)}, bf16[1032,256]{1,0:T(8,128)(2,1)}, u32[]{:S(2)}, u32[]{:S(2)}) collective-permute-start(bf16[1032,256]{1,0:T(8,128)(2,1)} %fusion.1.a0), channel_id=1, source_target_pairs={{0,1},{1,0},{2,3},{3,2},{4,5},{5,4},{6,7},{7,6},{8,9},{9,8},{10,11... | collective-permute-start | bytes 1585160 | tf_op jit(solution)/shard_map/ppermute | solution.py:32
  64.8 15.9 %collective-permute-start.4 = (bf16[1032,256]{1,0:T(8,128)(2,1)}, bf16[1032,256]{1,0:T(8,128)(2,1)}, u32[]{:S(2)}, u32[]{:S(2)}) collective-permute-start(bf16[1032,256]{1,0:T(8,128)(2,1)} %collective-permute-done.a1), channel_id=1, source_target_pairs={{0,1},{1,0},{2,3},{3,2},{4,5},{5,4},{6,7},{7,6},{8,9},{9,8},{10,11... | collective-permute-start | bytes 1585160 | tf_op jit(solution)/shard_map/ppermute | solution.py:32
  69.7 10.9 %collective-permute-start.5 = (bf16[1032,256]{1,0:T(8,128)(2,1)}, bf16[1032,256]{1,0:T(8,128)(2,1)}, u32[]{:S(2)}, u32[]{:S(2)}) collective-permute-start(bf16[1032,256]{1,0:T(8,128)(2,1)} %collective-permute-done.1.a2), channel_id=1, source_target_pairs={{0,1},{1,0},{2,3},{3,2},{4,5},{5,4},{6,7},{7,6},{8,9},{9,8},{10,11... | collective-permute-start | bytes 1585160 | tf_op jit(solution)/shard_map/ppermute | solution.py:32
  75.4 5.3 %collective-permute-start.6 = (bf16[1032,256]{1,0:T(8,128)(2,1)}, bf16[1032,256]{1,0:T(8,128)(2,1)}, u32[]{:S(2)}, u32[]{:S(2)}) collective-permute-start(bf16[1032,256]{1,0:T(8,128)(2,1)} %collective-permute-done.2.a3), channel_id=1, source_target_pairs={{0,1},{1,0},{2,3},{3,2},{4,5},{5,4},{6,7},{7,6},{8,9},{9,8},{10,11... | collective-permute-start | bytes 1585160 | tf_op jit(solution)/shard_map/ppermute | solution.py:32
  80.7 1.0 %copy-start = (f32[1024,128]{1,0:T(8,128)S(1)}, f32[1024,128]{1,0:T(8,128)}, u32[]{:S(2)}) copy-start(f32[1024,128]{1,0:T(8,128)} %get-tuple-element.9.sin_t) | copy-start | bytes 1572868
  81.7 1.0 %copy-start.1 = (f32[1024,128]{1,0:T(8,128)S(1)}, f32[1024,128]{1,0:T(8,128)}, u32[]{:S(2)}) copy-start(f32[1024,128]{1,0:T(8,128)} %get-tuple-element.10.cos_t) | copy-start | bytes 1572868
